TPU v7x, 32 devices: a whole 2x2x4 slice. The times are simulated.
32 devices in a mesh: sp: 8 (over z, x), tp: 4 (over y, core).
Axes of the slice: x: 2, y: 2, z: 4, core: 2. Of those that a mesh axis runs over, the one named last changes fastest.
Arguments:
- cotangent: bfloat16 [2048, 2048], P('sp', 'tp'), may hold values from -6 to 6
- moe_input: bfloat16 [2048, 2048], P('sp', 'tp'), may hold values from -6 to 6
- routes: int32 [2048, 2], P('sp'), may hold values from 0 to 7, all different within a row; in each aligned block of 256 rows (0 to 255, 256 to 511, ...) at most 96 rows name the same one
- gates: float32 [2048, 2], P('sp'), may hold values from 0.1 to 1
- w_gate: bfloat16 [8, 2048, 2048], P('sp', None, 'tp'), may hold values from -0.125 to 0.125
- w_up: bfloat16 [8, 2048, 2048], P('sp', None, 'tp'), may hold values from -0.125 to 0.125
- w_down: bfloat16 [8, 2048, 2048], P('sp', 'tp'), may hold values from -0.125 to 0.125
- out_proj: bfloat16 [1024, 2048], P('tp'), may hold values from -0.1875 to 0.1875
- conv_in: bfloat16 [1024, 2048], P('tp', 'sp'), may hold values from -6 to 6
- branch: bfloat16 [1024, 2048], P('tp', 'sp'), may hold values from -6 to 6
- state_before: float32 [1024, 2048], P('tp', 'sp'), may hold values from -6 to 6
- state_after: float32 [1024, 2048], P('tp', 'sp'), may hold values from -6 to 6
- jump: float32 [1024, 2048], P('tp', 'sp'), may hold values from -2 to 0, as said below
- recur_weight: bfloat16 [2, 16, 64, 64], P(None, 'tp'), may hold values from -0.75 to 0.75
- input_weight: bfloat16 [2, 16, 64, 64], P(None, 'tp'), may hold values from -0.75 to 0.75
- lam: float32 [2, 1024], P(None, 'tp')
Outputs:
- gate_grad: bfloat16 [8, 2048, 2048], P('sp', None, 'tp')
- up_grad: bfloat16 [8, 2048, 2048], P('sp', None, 'tp')
- down_grad: bfloat16 [8, 2048, 2048], P('sp', 'tp')
- residual_grad: bfloat16 [2048, 2048], P('sp', 'tp')
- out_proj_grad: float32 [1024, 2048], P('tp', 'sp')
- conv_grad: float32 [1024, 2048], P('tp', 'sp')
- branch_grad: float32 [1024, 2048], P('tp', 'sp')
Inputs may be any that keep to these rules, and one draw needn't show every extreme that they name: `routes`: each token names 2 different experts. Among the tokens of one index of sp (aligned blocks of 256 rows) no expert is named more than 96 times, a bound that some block reaches. `jump`: every entry is at most -1 / 20480.
All inputs are finite; a program needn't handle non-finite values.
Results may differ from a plain program's by a relative error of at most 0.02.
Values may be sent and summed in bfloat16 or wider, within the bound.
A program may use at most 128 MiB of HBM per device.

v0:
```python
import jax
import jax.numpy as jnp
from jax import lax
from jax.experimental import pallas as pl
from jax.experimental.pallas import tpu as pltpu
from jax.sharding import PartitionSpec as P

decay_scale = 8.0


MESH = pl.DeviceIdType.MESH
VMEM_SPEC = pl.BlockSpec(memory_space=pltpu.VMEM)


def at(sp=None, tp=None):
    sp = lax.axis_index("sp") if sp is None else sp
    tp = lax.axis_index("tp") if tp is None else tp
    return (sp, tp)


def meet(devices):
    barrier = pltpu.get_barrier_semaphore()
    for device in devices:
        pl.semaphore_signal(barrier, inc=1, device_id=device, device_id_type=MESH)
    pl.semaphore_wait(barrier, len(devices))


def remote(source, target, send, recv, device):
    return pltpu.make_async_remote_copy(
        src_ref=source, dst_ref=target, send_sem=send, recv_sem=recv,
        device_id=device, device_id_type=MESH,
    )


def params(collective_id):
    return pltpu.CompilerParams(
        collective_id=collective_id, has_side_effects=True, vmem_limit_bytes=48 * 1024 * 1024
    )


def dispatch(send_rows, send_grads):
    n, tp = lax.axis_size("sp"), lax.axis_size("tp")
    chips = tp // 2
    capacity, width = send_rows.shape[1:]
    groups = min(n, 8)
    span = n // groups

    def kernel(rows_ref, grads_ref, rows_out, grads_out, ss, sr, ps, pr, ys, yr, fs, fr):
        me, place = lax.axis_index("sp"), lax.axis_index("tp")
        chip, core = place // 2, place % 2
        partner = chip * 2 + (1 - core)
        group, inner = me // span, me % span
        pairs = ((rows_ref, rows_out), (grads_ref, grads_out))

        def columns(member):
            return pl.ds(pl.multiple_of(member * width, width), width)

        def peer(step, sign):
            other_group = lax.rem(group + sign * (step // span) + groups, groups)
            return other_group * span + lax.rem(inner + sign * (step % span) + span, span)

        def across(turn, sign):
            return lax.rem(chip + sign * turn + chips, chips) * 2 + core

        meet(
            [at(sp=peer(k, 1)) for k in range(1, n)]
            + [at(tp=partner)]
            + [at(tp=across(t, 1)) for t in range(1, chips)]
        )
        mine = columns(place)
        first = []
        for k in range(1, n):
            to = peer(k, 1)
            for kind, (source, out) in enumerate(pairs):
                copy = remote(
                    source.at[to], out.at[me, :, mine],
                    ss.at[k, kind], sr.at[k, kind], at(sp=to),
                )
                copy.start()
                first.append(copy)
        for source, out in pairs:
            out[me, :, mine] = source[me]
        sent = []
        for g in range(groups):
            base = lax.rem(group - g + groups, groups) * span
            for kind, (source, out) in enumerate(pairs):
                for i in range(span):
                    k = g * span + i
                    if k == 0:
                        continue
                    origin = peer(k, -1)
                    remote(
                        source.at[origin], out.at[origin, :, mine],
                        ss.at[k, kind], sr.at[k, kind], at(sp=origin),
                    ).wait_recv()
                block = out.at[pl.ds(base, span), :, mine]
                if g == 0 and span == 1:
                    block = source.at[pl.ds(base, span)]
                landing = out.at[pl.ds(base, span), :, mine]
                for t in range(1, chips):
                    copy = remote(
                        block, landing, ys.at[g, t, kind], yr.at[g, t, kind], at(tp=across(t, 1))
                    )
                    copy.start()
                    sent.append(copy)
                copy = remote(block, landing, ps.at[g, kind], pr.at[g, kind], at(tp=partner))
                copy.start()
                sent.append(copy)
        for g in range(groups):
            base = lax.rem(group - g + groups, groups) * span
            for kind, (source, out) in enumerate(pairs):
                for t in range(1, chips):
                    block = out.at[pl.ds(base, span), :, columns(across(t, -1))]
                    remote(
                        block, block, ys.at[g, t, kind], yr.at[g, t, kind], at(tp=across(t, -1))
                    ).wait_recv()
                    copy = remote(
                        block, block, fs.at[g, t, kind], fr.at[g, t, kind], at(tp=partner)
                    )
                    copy.start()
                    sent.append(copy)
        for g in range(groups):
            base = lax.rem(group - g + groups, groups) * span
            for kind, (source, out) in enumerate(pairs):
                block = out.at[pl.ds(base, span), :, columns(partner)]
                remote(block, block, ps.at[g, kind], pr.at[g, kind], at(tp=partner)).wait_recv()
                for t in range(1, chips):
                    member = lax.rem(chip - t + chips, chips) * 2 + (1 - core)
                    block = out.at[pl.ds(base, span), :, columns(member)]
                    remote(
                        block, block, fs.at[g, t, kind], fr.at[g, t, kind], at(tp=partner)
                    ).wait_recv()
        for copy in first + sent:
            copy.wait_send()

    full = jax.ShapeDtypeStruct((n, capacity, tp * width), send_rows.dtype)
    dma = pltpu.SemaphoreType.DMA
    sems = [dma((n, 2))] * 2 + [dma((groups, 2))] * 2 + [dma((groups, max(chips, 2), 2))] * 4
    return pl.pallas_call(
        kernel, name="dispatch", out_shape=(full, full),
        in_specs=[VMEM_SPEC] * 2, out_specs=(VMEM_SPEC,) * 2,
        scratch_shapes=sems, compiler_params=params(1),
    )(send_rows, send_grads)


def scatter_sum(partial):
    tp = lax.axis_size("tp")
    chips = tp // 2
    rows, full = partial.shape
    width = full // tp
    strip = 32

    def kernel(part_ref, out_ref, near, total, far, own, ns, nr, ys, yr):
        place = lax.axis_index("tp")
        chip, core = place // 2, place % 2
        partner = chip * 2 + (1 - core)

        def columns(member):
            return pl.ds(pl.multiple_of(member * width, width), width)

        def turned(t, sign):
            return lax.rem(chip + sign * t + chips, chips)

        meet([at(tp=partner)] + [at(tp=turned(t, 1) * 2 + core) for t in range(1, chips)])
        order = list(range(1, chips)) + [0]
        copies = []
        for t in order:
            copy = remote(
                part_ref.at[:, columns(turned(t, 1) * 2 + (1 - core))],
                near.at[t], ns.at[t], nr.at[t], at(tp=partner),
            )
            copy.start()
            copies.append(copy)
        for t, copy in zip(order, copies):
            copy.wait_recv()
            mine = columns(turned(t, 1) * 2 + core)

            @pl.loop(0, rows // strip)
            def _(i):
                where = pl.ds(pl.multiple_of(i * strip, strip), strip)
                value = part_ref[where, mine].astype(jnp.float32) + near[t, where].astype(
                    jnp.float32
                )
                if t == 0:
                    own[where] = value
                else:
                    total[t, where] = value.astype(total.dtype)

        sends = []
        for t in range(1, chips):
            copy = remote(
                total.at[t], far.at[t], ys.at[t], yr.at[t], at(tp=turned(t, 1) * 2 + core)
            )
            copy.start()
            sends.append(copy)
        for copy in sends:
            copy.wait_recv()

        @pl.loop(0, rows // strip)
        def _(i):
            where = pl.ds(pl.multiple_of(i * strip, strip), strip)
            value = own[where]
            for t in range(1, chips):
                value = value + far[t, where].astype(jnp.float32)
            out_ref[where] = value.astype(out_ref.dtype)

        for copy in copies + sends:
            copy.wait_send()

    dma = pltpu.SemaphoreType.DMA
    block = pltpu.VMEM((chips, rows, width), partial.dtype)
    return pl.pallas_call(
        kernel, name="scatter_sum",
        out_shape=jax.ShapeDtypeStruct((rows, width), partial.dtype),
        in_specs=[VMEM_SPEC], out_specs=VMEM_SPEC,
        scratch_shapes=[block, block, block, pltpu.VMEM((rows, width), jnp.float32)]
        + [dma((chips,))] * 4,
        compiler_params=params(2),
    )(partial)


def share(values):
    n = lax.axis_size("sp")

    def kernel(in_ref, out_ref, ss, sr):
        me = lax.axis_index("sp")
        meet([at(sp=lax.rem(me + k, n)) for k in range(1, n)])
        copies = []
        for k in range(1, n):
            copy = remote(
                in_ref, out_ref.at[me], ss.at[k], sr.at[k], at(sp=lax.rem(me + k, n))
            )
            copy.start()
            copies.append(copy)
        out_ref[me] = in_ref[...]
        for k in range(1, n):
            origin = lax.rem(me - k + n, n)
            remote(in_ref, out_ref.at[origin], ss.at[k], sr.at[k], at(sp=origin)).wait_recv()
        for copy in copies:
            copy.wait_send()

    dma = pltpu.SemaphoreType.DMA
    return pl.pallas_call(
        kernel, name="share",
        out_shape=jax.ShapeDtypeStruct((n,) + values.shape, values.dtype),
        in_specs=[VMEM_SPEC], out_specs=VMEM_SPEC,
        scratch_shapes=[dma((n,))] * 2, compiler_params=params(3),
    )(values)


def silu_parts(pre_act):
    sigmoid_val = jax.nn.sigmoid(pre_act)
    return (pre_act * sigmoid_val, sigmoid_val * (1.0 + pre_act * (1.0 - sigmoid_val)))


def block_map(values, weight):
    return jnp.einsum("nit,nij->njt", values, weight, preferred_element_type=jnp.float32)


def block_back(gradient, weight):
    return jnp.einsum(
        "njt,nij->nit", gradient, weight.astype(jnp.float32), precision=lax.Precision.HIGHEST
    )


def gate_values(conv_in, weight_r, weight_i, lam_row, jump):
    channels, length = conv_in.shape
    shaped = conv_in.reshape(weight_r.shape[0], weight_r.shape[1], length)
    recur_gate = jax.nn.sigmoid(block_map(shaped, weight_r).reshape(channels, length))
    inward = jax.nn.sigmoid(block_map(shaped, weight_i).reshape(channels, length))
    speed_row = decay_scale * jax.nn.softplus(-lam_row)[:, None]
    log_decay = -speed_row * recur_gate + jump
    retain = jnp.exp(log_decay)
    root_term = jnp.sqrt(-jnp.expm1(2.0 * log_decay))
    conv_wide = conv_in.astype(jnp.float32)
    return (recur_gate, inward, speed_row, retain, root_term, conv_wide)


def gate_backward(pieces, decay_grad, drive_grad, weight_r, weight_i):
    recur_gate, inward, speed_row, retain, root_term, conv_wide = pieces
    channels, length = conv_wide.shape
    shape_three = (weight_r.shape[0], weight_r.shape[1], length)
    log_grad = decay_grad * retain - drive_grad * inward * conv_wide * retain * retain / root_term
    recur_grad = log_grad * -speed_row * recur_gate * (1.0 - recur_gate)
    inward_grad = drive_grad * root_term * conv_wide * inward * (1.0 - inward)
    direct = drive_grad * root_term * inward
    back_r = block_back(recur_grad.reshape(shape_three), weight_r)
    back_i = block_back(inward_grad.reshape(shape_three), weight_i)
    return direct + (back_r + back_i).reshape(channels, length)


def combine_pair(earlier, latter):
    return (earlier[0] * latter[0], latter[0] * earlier[1] + latter[1])


def expert_pass(full_rows, full_grads, gate_weight, up_weight, down_weight):
    contract_last = (((1,), (1,)), ((), ()))
    contract_first = (((0,), (0,)), ((), ()))
    pre_gate = jnp.dot(full_rows, gate_weight, preferred_element_type=jnp.float32)
    pre_up = jnp.dot(full_rows, up_weight, preferred_element_type=jnp.float32)
    silu_val, silu_slope = silu_parts(pre_gate)
    activation = (silu_val * pre_up).astype(jnp.bfloat16)
    act_grad = lax.dot_general(
        full_grads, down_weight, contract_last, preferred_element_type=jnp.float32
    )
    up_hidden = (act_grad * silu_val).astype(jnp.bfloat16)
    gate_hidden = (act_grad * pre_up * silu_slope).astype(jnp.bfloat16)
    partial_value = lax.dot_general(
        gate_hidden, gate_weight, contract_last, preferred_element_type=jnp.float32
    )
    partial_value = (
        partial_value
        + lax.dot_general(up_hidden, up_weight, contract_last, preferred_element_type=jnp.float32)
    ).astype(jnp.bfloat16)
    gate_acc = lax.dot_general(
        full_rows, gate_hidden, contract_first, preferred_element_type=jnp.float32
    )
    up_acc = lax.dot_general(
        full_rows, up_hidden, contract_first, preferred_element_type=jnp.float32
    )
    down_acc = lax.dot_general(
        activation, full_grads, contract_first, preferred_element_type=jnp.float32
    )
    return (partial_value, (gate_acc, up_acc, down_acc))


def on_device(
    cotangent,
    moe_input,
    routes,
    gates,
    w_gate,
    w_up,
    w_down,
    out_proj,
    conv_in,
    branch,
    state_before,
    state_after,
    jump,
    recur_weight,
    input_weight,
    lam,
):
    tokens_dev, width_dev = cotangent.shape
    per_token = routes.shape[1]
    experts = lax.axis_size("sp")
    capacity = 3 * tokens_dev // experts
    pair_total = tokens_dev * per_token
    routed = routes.reshape(-1)
    onehot = (routed[:, None] == jnp.arange(experts, dtype=jnp.int32)[None, :]).astype(jnp.int32)
    earlier_count = jnp.cumsum(onehot, axis=0) - onehot
    token_position = jnp.sum(earlier_count * onehot, axis=1)
    target = routed * capacity + token_position
    scaled = (cotangent.astype(jnp.float32)[:, None, :] * gates[:, :, None]).astype(jnp.bfloat16)
    scaled = scaled.reshape(pair_total, width_dev)
    copies = jnp.broadcast_to(moe_input[:, None, :], (tokens_dev, per_token, width_dev)).reshape(
        pair_total, width_dev
    )
    blank = jnp.zeros((experts * capacity, width_dev), jnp.bfloat16)
    send_rows = blank.at[target].set(copies).reshape(experts, capacity, width_dev)
    send_grads = blank.at[target].set(scaled).reshape(experts, capacity, width_dev)
    total_rows = experts * capacity
    full_rows, full_grads = dispatch(send_rows, send_grads)
    full_rows = full_rows.reshape(total_rows, -1)
    full_grads = full_grads.reshape(total_rows, -1)
    partial_value, totals = expert_pass(full_rows, full_grads, w_gate[0], w_up[0], w_down[0])
    row_grad = scatter_sum(partial_value)
    gate_grad = totals[0].astype(jnp.bfloat16)[None]
    up_grad = totals[1].astype(jnp.bfloat16)[None]
    down_grad = totals[2].astype(jnp.bfloat16)[None]
    returned = lax.all_to_all(
        row_grad.reshape(experts, capacity, width_dev),
        "sp",
        split_axis=0,
        concat_axis=0,
        tiled=True,
    )
    returned = returned.reshape(experts * capacity, width_dev)[target].reshape(
        tokens_dev, per_token, width_dev
    )
    residual_grad = (
        cotangent.astype(jnp.float32) + jnp.sum(returned.astype(jnp.float32), axis=1)
    ).astype(jnp.bfloat16)
    full_residual = lax.all_gather(residual_grad, "tp", axis=1, tiled=True)
    pieces_fwd = gate_values(conv_in, recur_weight[0], input_weight[0], lam[0], jump)
    pieces_bwd = gate_values(conv_in, recur_weight[1], input_weight[1], lam[1], jump)
    drive_fwd = pieces_fwd[4] * pieces_fwd[1] * pieces_fwd[5]
    drive_bwd = pieces_bwd[4] * pieces_bwd[1] * pieces_bwd[5]
    lru_out = pieces_fwd[3] * state_before + drive_fwd + pieces_bwd[3] * state_after + drive_bwd
    gelu_val, gelu_back = jax.vjp(jax.nn.gelu, branch.astype(jnp.float32))
    mix = (lru_out * gelu_val).astype(jnp.bfloat16)
    proj_part = lax.dot_general(
        full_residual, mix, (((0,), (1,)), ((), ())), preferred_element_type=jnp.float32
    ).astype(jnp.bfloat16)
    proj_part, full_residual = lax.optimization_barrier((proj_part, full_residual))
    proj_rows = lax.psum_scatter(proj_part, "sp", scatter_dimension=0, tiled=True).astype(
        jnp.float32
    )
    out_proj_grad = proj_rows.T
    mix_grad = lax.dot_general(
        out_proj, full_residual, (((1,), (1,)), ((), ())), preferred_element_type=jnp.float32
    )
    lru_grad = mix_grad * gelu_val
    branch_grad = gelu_back(mix_grad * lru_out)[0]
    decay_fwd = pieces_fwd[3]
    decay_bwd = pieces_bwd[3]
    prod_fwd, local_fwd = lax.associative_scan(
        combine_pair, (decay_fwd, decay_fwd * lru_grad), reverse=True, axis=1
    )
    prod_bwd, local_bwd = lax.associative_scan(
        combine_pair, (decay_bwd, decay_bwd * lru_grad), axis=1
    )
    ends = jnp.concatenate([prod_fwd[:, 0], local_fwd[:, 0], prod_bwd[:, -1], local_bwd[:, -1]])
    shared = share(ends[None]).reshape(experts, 4, -1)
    place = lax.axis_index("sp")
    incoming_fwd = jnp.zeros_like(local_fwd[:, 0])
    incoming_bwd = jnp.zeros_like(incoming_fwd)
    for turn in range(experts - 1):
        late = experts - 1 - turn
        incoming_fwd = jnp.where(
            late > place, shared[late, 0] * incoming_fwd + shared[late, 1], incoming_fwd
        )
        incoming_bwd = jnp.where(
            turn < place, shared[turn, 2] * incoming_bwd + shared[turn, 3], incoming_bwd
        )
    carried_fwd = local_fwd + prod_fwd * incoming_fwd[:, None]
    carried_bwd = local_bwd + prod_bwd * incoming_bwd[:, None]
    delta_fwd = lru_grad + jnp.concatenate([carried_fwd[:, 1:], incoming_fwd[:, None]], axis=1)
    delta_bwd = lru_grad + jnp.concatenate([incoming_bwd[:, None], carried_bwd[:, :-1]], axis=1)
    conv_grad = gate_backward(
        pieces_fwd, delta_fwd * state_before, delta_fwd, recur_weight[0], input_weight[0]
    )
    conv_grad = conv_grad + gate_backward(
        pieces_bwd, delta_bwd * state_after, delta_bwd, recur_weight[1], input_weight[1]
    )
    return (gate_grad, up_grad, down_grad, residual_grad, out_proj_grad, conv_grad, branch_grad)


def solution(mesh):
    placed = (
        P("sp", "tp"),
        P("sp", "tp"),
        P("sp", None),
        P("sp", None),
        P("sp", None, "tp"),
        P("sp", None, "tp"),
        P("sp", "tp", None),
        P("tp", None),
        P("tp", "sp"),
        P("tp", "sp"),
        P("tp", "sp"),
        P("tp", "sp"),
        P("tp", "sp"),
        P(None, "tp", None, None),
        P(None, "tp", None, None),
        P(None, "tp"),
    )
    return jax.shard_map(
        on_device,
        mesh=mesh,
        in_specs=placed,
        out_specs=(
            P("sp", None, "tp"),
            P("sp", None, "tp"),
            P("sp", "tp", None),
            P("sp", "tp"),
            P("tp", "sp"),
            P("tp", "sp"),
            P("tp", "sp"),
        ),
        check_vma=False,
    )
```

profile of v0, /device:TPU:0, one launch (start us, length us, event | category | flops | bytes accessed | tf_op | source)
XLA Modules:
  0.0 269.6 jit_solution(8960910477145036209)
XLA Ops:
  9.4 1.1 reduce-window.6
  10.8 1.2 broadcast_in_dim.13
  12.1 1.0 reshape.583
  13.4 1.7 mul.648
  15.4 3.8 %scatter_custom_fusion = bf16[768,512]{1,0:T(8,128)(2,1)} fusion(s32[512]{0:T(512)S(1)} %bitcast.326, bf16[512,512]{1,0:T(8,128)(2,1)} %reshape.583, bf16[]{:T(256)} %constant.22.clone.1), kind=kCustom, calls=%fused_computation.62 | custom fusion | bytes 786944 | tf_op jit(solution)/shard_map/scatter | solution.py:361
  19.3 3.5 %scatter_custom_fusion.1 = bf16[768,512]{1,0:T(8,128)(2,1)S(1)} fusion(s32[512]{0:T(512)S(1)} %bitcast.327, f32[512,512]{1,0:T(8,128)} %mul.648, f32[512]{0:T(512)S(1)} %mul.649, bf16[]{:T(256)} %constant.22.clone.1), kind=kCustom, calls=%fused_computation.51 | custom fusion | flops 524288 | bytes 1837058 | tf_op jit(solution)/shard_map/scatter | solution.py:362
  22.8 1.1 copy-done.2
  23.9 53.9 %dispatch.1 = (bf16[8,96,2048]{2,1,0:T(8,128)(2,1)S(1)}, bf16[8,96,2048]{2,1,0:T(8,128)(2,1)}) custom-call(bf16[8,96,512]{2,1,0:T(8,128)(2,1)S(1)} %bitcast.305, bf16[8,96,512]{2,1,0:T(8,128)(2,1)S(1)} %bitcast.304), custom_call_target="tpu_custom_call" | custom-call | tf_op jit(solution)/shard_map/dispatch/pallas_call | solution.py:139
  77.9 1.8 fusion.5
  80.6 1.8 fusion.8
  83.0 1.2 copy-done.50
  84.2 2.3 multiply_convert_fusion.1
  86.6 1.8 fusion.3
  88.4 1.8 add_convert_fusion.part_ref
  90.3 24.7 %scatter_sum.1 = bf16[768,512]{1,0:T(8,128)(2,1)} custom-call(bf16[768,2048]{1,0:T(8,128)(2,1)S(1)} %add_convert_fusion.part_ref), custom_call_target="tpu_custom_call" | custom-call | tf_op jit(solution)/shard_map/scatter_sum/pallas_call | solution.py:212
  115.0 12.1 %all-to-all-start = ((bf16[8,96,512]{2,1,0:T(8,128)(2,1)}), bf16[8,96,512]{2,1,0:T(8,128)(2,1)S(1)}, u32[]{:S(2)}, u32[]{:S(2)}) async-start(bf16[8,96,512]{2,1,0:T(8,128)(2,1)} %bitcast.14), calls=%async_computation | async-start | bytes 1572864 | tf_op jit(solution)/shard_map/all_to_all | solution.py:372
  131.6 1.0 fusion.117
  132.6 14.6 %all-to-all-done = bf16[8,96,512]{2,1,0:T(8,128)(2,1)S(1)} async-done(((bf16[8,96,512]{2,1,0:T(8,128)(2,1)}), bf16[8,96,512]{2,1,0:T(8,128)(2,1)S(1)}, u32[]{:S(2)}, u32[]{:S(2)}) %all-to-all-start) | async-done | bytes 786464 | tf_op jit(solution)/shard_map/all_to_all | solution.py:372
  147.2 2.0 gather_fusion
  149.9 1.2 reduce_sum.22
  152.2 2.5 fusion.51
  154.7 1.6 slice.738
  156.4 1.6 slice.703
  158.0 1.6 slice.704
  160.3 1.6 slice.630
  161.9 1.6 slice.623
  163.5 1.6 slice.621
  165.8 1.7 copy.81
  167.4 1.5 slice.631
  168.9 1.5 slice.624
  170.4 1.5 slice.622
  172.0 4.4 %fusion = bf16[1,2048,512]{2,1,0:T(8,128)(2,1)} fusion(bf16[768,2048]{1,0:T(8,128)(2,1)S(1)} %bitcast.309, bf16[768,512]{1,0:T(8,128)(2,1)} %copy-done.21), kind=kOutput, calls=%fused_computation.7 | convolution fusion | flops 1611661312 | bytes 6029312 | tf_op jit(solution)/shard_map/dot_general | solution.py:315
  176.3 3.2 %fusion.1 = bf16[1,2048,512]{2,1,0:T(8,128)(2,1)} fusion(bf16[768,2048]{1,0:T(8,128)(2,1)S(1)} %bitcast.310, bf16[768,512]{1,0:T(8,128)(2,1)S(1)} %copy-done.20), kind=kOutput, calls=%fused_computation.8 | convolution fusion | flops 1611661312 | bytes 6029312 | tf_op jit(solution)/shard_map/dot_general | solution.py:318
  179.5 3.3 %fusion.2 = bf16[1,512,2048]{2,1,0:T(8,128)(2,1)} fusion(bf16[768,2048]{1,0:T(8,128)(2,1)S(1)} %bitcast.363, f32[768,512]{1,0:T(8,128)S(1)} %copy-done.55, f32[768,512]{1,0:T(8,128)S(1)} %copy-done.53), kind=kOutput, calls=%fused_computation.9 | convolution fusion | flops 1614020608 | bytes 8388608 | tf_op jit(solution)/shard_map/dot_general | solution.py:321
  182.9 2.9 %convolution_convert_fusion.3 = bf16[2048,256]{1,0:T(8,128)(2,1)} fusion(bf16[256,2048]{1,0:T(8,128)(2,1)} %all-gather.2.cloned.1.call-done, f32[256,256]{0,1:T(8,128)S(1)} %copy-done.29, bf16[256,256]{0,1:T(8,128)(2,1)S(1)} %copy-done.38), kind=kOutput, calls=%fused_computation.10 | convolution fusion | flops 269680640 | bytes 2490368 | tf_op jit(solution)/shard_map/dot_general | solution.py:393
  185.8 2.6 exponential_multiply_fusion.1
  191.6 1.5 pad.258
  193.8 1.4 pad.242
  201.6 6.7 %share.1 = f32[8,1,1024]{2,1,0:T(1,128)S(1)} custom-call(f32[1,1024]{1,0:T(1,128)S(1)} %bitcast.306), custom_call_target="tpu_custom_call" | custom-call | tf_op jit(solution)/shard_map/share/pallas_call | solution.py:243
  209.2 1.1 fusion.55
  210.8 1.1 copy.103
  211.9 1.1 convolution_add_fusion
  214.4 1.0 fusion.53
  216.0 1.0 convolution_add_fusion.1
  217.0 1.2 copy.93
  218.2 1.1 add_add_fusion
  220.2 1.8 copy.108
  222.0 39.1 %reduce-scatter.2.cloned.1.call-done = bf16[256,256]{1,0:T(8,128)(2,1)} async-done(((bf16[2048,256]{1,0:T(8,128)(2,1)}), bf16[256,256]{1,0:T(8,128)(2,1)}) %reduce-scatter.2.cloned.1.call-update) | async-done | bytes 131088 | tf_op jit(solution)/shard_map/reduce_scatter | solution.py:397
  (420 shorter events, 26.9 us)
Async XLA Ops:
  7.2 70.7 %copy-start = (bf16[1,2048,512]{2,1,0:T(8,128)(2,1)S(1)}, bf16[1,2048,512]{2,1,0:T(8,128)(2,1)}, u32[]{:S(2)}) copy-start(bf16[1,2048,512]{2,1,0:T(8,128)(2,1)} %param.20) | copy-start | bytes 6291460
  7.2 5.9 %copy-start.17 = (bf16[256,512]{1,0:T(8,128)(2,1)S(1)}, bf16[256,512]{1,0:T(8,128)(2,1)}, u32[]{:S(2)}) copy-start(bf16[256,512]{1,0:T(8,128)(2,1)} %param.16) | copy-start | bytes 786436
  12.1 3.0 %copy-start.46 = (f32[256,2]{0,1:T(2,128)S(1)}, f32[256,2]{0,1:T(2,128)}, u32[]{:S(2)}) copy-start(f32[256,2]{0,1:T(2,128)} %param.19) | copy-start | bytes 6148
  77.8 2.7 %copy-start.14 = (bf16[1,2048,512]{2,1,0:T(8,128)(2,1)S(1)}, bf16[1,2048,512]{2,1,0:T(8,128)(2,1)}, u32[]{:S(2)}) copy-start(bf16[1,2048,512]{2,1,0:T(8,128)(2,1)} %param.21) | copy-start | bytes 6291460
  80.6 2.5 copy-start.48
  80.6 3.7 %copy-start.50 = (bf16[1,512,2048]{2,1,0:T(8,128)(2,1)S(1)}, bf16[1,512,2048]{2,1,0:T(8,128)(2,1)}, u32[]{:S(2)}) copy-start(bf16[1,512,2048]{2,1,0:T(8,128)(2,1)} %param.22) | copy-start | bytes 6291460
  82.4 4.2 %copy-start.54 = (f32[768,512]{1,0:T(8,128)}, f32[768,512]{1,0:T(8,128)S(1)}, u32[]{:S(2)}) copy-start(f32[768,512]{1,0:T(8,128)S(1)} %fusion.8) | copy-start | bytes 4718596
  86.5 1.9 copy-start.21
  90.3 36.9 %copy-start.37 = (bf16[256,256]{1,0:T(8,128)(2,1)S(1)}, bf16[256,256]{1,0:T(8,128)(2,1)}, u32[]{:S(2)}) copy-start(bf16[256,256]{1,0:T(8,128)(2,1)} %param.24) | copy-start | bytes 393220
  90.3 36.9 %copy-start.39 = (bf16[2,4,64,64]{3,2,1,0:T(8,128)(2,1)S(1)}, bf16[2,4,64,64]{3,2,1,0:T(8,128)(2,1)}, u32[]{:S(2)}) copy-start(bf16[2,4,64,64]{3,2,1,0:T(8,128)(2,1)} %param.30) | copy-start | bytes 196612
  115.0 13.0 %copy-start.30 = (f32[256,256]{1,0:T(8,128)S(1)}, f32[256,256]{1,0:T(8,128)}, u32[]{:S(2)}) copy-start(f32[256,256]{1,0:T(8,128)} %param.27) | copy-start | bytes 786436
  115.0 32.3 %all-to-all-start = ((bf16[8,96,512]{2,1,0:T(8,128)(2,1)}), bf16[8,96,512]{2,1,0:T(8,128)(2,1)S(1)}, u32[]{:S(2)}, u32[]{:S(2)}) async-start(bf16[8,96,512]{2,1,0:T(8,128)(2,1)} %bitcast.14), calls=%async_computation | async-start | bytes 1572864 | tf_op jit(solution)/shard_map/all_to_all | solution.py:372
  127.1 2.6 copy-start.31
  127.1 55.8 %all-gather.2.cloned.1.call-start = ((), (), s32[]{:S(2)}) async-start(), calls=%async_computation.2 | async-start | bytes 1310720 | tf_op jit(solution)/shard_map/all_gather | solution.py:385
  127.2 3.3 %copy-start.32 = (f32[256,256]{1,0:T(8,128)S(1)}, f32[256,256]{1,0:T(8,128)}, u32[]{:S(2)}) copy-start(f32[256,256]{1,0:T(8,128)} %param.28) | copy-start | bytes 786436
  127.4 3.2 %copy-start.35 = (bf16[2,4,64,64]{3,2,1,0:T(8,128)(2,1)S(1)}, bf16[2,4,64,64]{3,2,1,0:T(8,128)(2,1)}, u32[]{:S(2)}) copy-start(bf16[2,4,64,64]{3,2,1,0:T(8,128)(2,1)} %param.29) | copy-start | bytes 196612
  131.1 18.1 %copy-start.12 = (f32[256,256]{0,1:T(8,128)}, f32[256,256]{0,1:T(8,128)S(1)}, u32[]{:S(2)}) copy-start(f32[256,256]{0,1:T(8,128)S(1)} %copy.76) | copy-start | bytes 786436
  131.5 15.7 %copy-start.10 = (f32[256,256]{0,1:T(8,128)}, f32[256,256]{0,1:T(8,128)S(1)}, u32[]{:S(2)}) copy-start(f32[256,256]{0,1:T(8,128)S(1)} %copy.69) | copy-start | bytes 786436
  149.2 1.9 copy-start.18
  151.9 109.1 %reduce-scatter.2.cloned.1.call-start = ((), (), s32[]{:S(2)}) async-start(), calls=%async_computation.3 | async-start | bytes 1179648 | tf_op jit(solution)/shard_map/reduce_scatter | solution.py:397
  152.2 19.8 %copy-start.4 = (bf16[8,96,2048]{2,1,0:T(8,128)(2,1)S(1)}, bf16[8,96,2048]{2,1,0:T(8,128)(2,1)}, u32[]{:S(2)}) copy-start(bf16[8,96,2048]{2,1,0:T(8,128)(2,1)} %copy-done.3) | copy-start | bytes 9437188
  172.0 4.4 %copy-start.20 = (bf16[768,512]{1,0:T(8,128)(2,1)S(1)}, bf16[768,512]{1,0:T(8,128)(2,1)}, u32[]{:S(2)}) copy-start(bf16[768,512]{1,0:T(8,128)(2,1)} %copy-done.19) | copy-start | bytes 2359300
  176.3 3.2 %copy-start.49 = (bf16[8,96,2048]{2,1,0:T(8,128)(2,1)S(1)}, bf16[8,96,2048]{2,1,0:T(8,128)(2,1)}, u32[]{:S(2)}) copy-start(bf16[8,96,2048]{2,1,0:T(8,128)(2,1)} %get-tuple-element.12) | copy-start | bytes 9437188
  176.3 3.2 %copy-start.53 = (f32[768,512]{1,0:T(8,128)S(1)}, f32[768,512]{1,0:T(8,128)}, u32[]{:S(2)}) copy-start(f32[768,512]{1,0:T(8,128)} %copy-done.52) | copy-start | bytes 4718596
  176.3 3.2 %copy-start.55 = (f32[768,512]{1,0:T(8,128)S(1)}, f32[768,512]{1,0:T(8,128)}, u32[]{:S(2)}) copy-start(f32[768,512]{1,0:T(8,128)} %copy-done.54) | copy-start | bytes 4718596
  179.5 3.3 %copy-start.29 = (f32[256,256]{0,1:T(8,128)S(1)}, f32[256,256]{0,1:T(8,128)}, u32[]{:S(2)}) copy-start(f32[256,256]{0,1:T(8,128)} %fusion.51) | copy-start | bytes 786436
  179.5 3.3 %copy-start.38 = (bf16[256,256]{0,1:T(8,128)(2,1)S(1)}, bf16[256,256]{0,1:T(8,128)(2,1)}, u32[]{:S(2)}) copy-start(bf16[256,256]{0,1:T(8,128)(2,1)} %copy.81) | copy-start | bytes 393220
  182.8 2.9 %copy-start.9 = (f32[256,256]{0,1:T(8,128)S(1)}, f32[256,256]{0,1:T(8,128)}, u32[]{:S(2)}) copy-start(f32[256,256]{0,1:T(8,128)} %get-tuple-element.49) | copy-start | bytes 786436
  182.8 2.9 %copy-start.51 = (bf16[256,2048]{1,0:T(8,128)(2,1)S(1)}, bf16[256,2048]{1,0:T(8,128)(2,1)}, u32[]{:S(2)}) copy-start(bf16[256,2048]{1,0:T(8,128)(2,1)} %param.23) | copy-start | bytes 3145732
  185.7 2.6 copy-start.6
  185.8 2.9 %copy-start.25 = (f32[256,128]{0,1:T(8,128)S(1)}, f32[256,128]{0,1:T(8,128)}, u32[]{:S(2)}) copy-start(f32[256,128]{0,1:T(8,128)} %slice.703) | copy-start | bytes 393220
  185.8 2.9 %copy-start.26 = (f32[256,128]{0,1:T(8,128)S(1)}, f32[256,128]{0,1:T(8,128)}, u32[]{:S(2)}) copy-start(f32[256,128]{0,1:T(8,128)} %slice.704) | copy-start | bytes 393220
  191.5 4.2 %copy-start.23 = (f32[256,128]{0,1:T(8,128)S(1)}, f32[256,128]{0,1:T(8,128)}, u32[]{:S(2)}) copy-start(f32[256,128]{0,1:T(8,128)} %slice.631) | copy-start | bytes 393220
  191.5 4.2 %copy-start.24 = (f32[256,128]{0,1:T(8,128)S(1)}, f32[256,128]{0,1:T(8,128)}, u32[]{:S(2)}) copy-start(f32[256,128]{0,1:T(8,128)} %slice.624) | copy-start | bytes 393220
  198.5 10.6 %copy-start.8 = (f32[256,256]{0,1:T(8,128)S(1)}, f32[256,256]{0,1:T(8,128)}, u32[]{:S(2)}) copy-start(f32[256,256]{0,1:T(8,128)} %copy.78) | copy-start | bytes 786436
  198.5 10.6 %copy-start.13 = (f32[256,256]{0,1:T(8,128)S(1)}, f32[256,256]{0,1:T(8,128)}, u32[]{:S(2)}) copy-start(f32[256,256]{0,1:T(8,128)} %copy-done.12) | copy-start | bytes 786436
  208.4 2.1 copy-start.33
  210.3 3.9 %copy-start.41 = (f32[1,1,256]{2,1,0:T(1,128)S(1)}, f32[1,1,256]{2,1,0:T(1,128)}, u32[]{:S(2)}) copy-start(f32[1,1,256]{2,1,0:T(1,128)} %get-tuple-element.79) | copy-start | bytes 3076
  210.3 3.9 %copy-start.42 = (f32[1,1,256]{2,1,0:T(1,128)S(1)}, f32[1,1,256]{2,1,0:T(1,128)}, u32[]{:S(2)}) copy-start(f32[1,1,256]{2,1,0:T(1,128)} %get-tuple-element.80) | copy-start | bytes 3076
  210.3 3.9 %copy-start.43 = (f32[1,1,256]{2,1,0:T(1,128)S(1)}, f32[1,1,256]{2,1,0:T(1,128)}, u32[]{:S(2)}) copy-start(f32[1,1,256]{2,1,0:T(1,128)} %get-tuple-element.81) | copy-start | bytes 3076
  210.3 3.9 %copy-start.44 = (f32[1,1,256]{2,1,0:T(1,128)S(1)}, f32[1,1,256]{2,1,0:T(1,128)}, u32[]{:S(2)}) copy-start(f32[1,1,256]{2,1,0:T(1,128)} %get-tuple-element.82) | copy-start | bytes 3076
  210.4 3.9 %copy-start.45 = (f32[1,1,256]{2,1,0:T(1,128)S(1)}, f32[1,1,256]{2,1,0:T(1,128)}, u32[]{:S(2)}) copy-start(f32[1,1,256]{2,1,0:T(1,128)} %get-tuple-element.83) | copy-start | bytes 3076
  210.5 3.6 %copy-start.34 = (f32[8,4,256]{2,1,0:T(4,128)S(1)}, f32[8,4,256]{2,1,0:T(4,128)}, u32[]{:S(2)}) copy-start(f32[8,4,256]{2,1,0:T(4,128)} %copy-done.33) | copy-start | bytes 98308
  210.5 3.8 %copy-start.5 = (f32[256,256]{0,1:T(8,128)S(1)}, f32[256,256]{0,1:T(8,128)}, u32[]{:S(2)}) copy-start(f32[256,256]{0,1:T(8,128)} %copy.73) | copy-start | bytes 786436
  210.5 3.8 %copy-start.7 = (f32[256,256]{0,1:T(8,128)S(1)}, f32[256,256]{0,1:T(8,128)}, u32[]{:S(2)}) copy-start(f32[256,256]{0,1:T(8,128)} %copy.71) | copy-start | bytes 786436
  210.6 3.8 %copy-start.11 = (f32[256,256]{0,1:T(8,128)S(1)}, f32[256,256]{0,1:T(8,128)}, u32[]{:S(2)}) copy-start(f32[256,256]{0,1:T(8,128)} %copy-done.10) | copy-start | bytes 786436
  215.4 2.8 %copy-start.16 = (f32[256,256]{0,1:T(8,128)S(1)}, f32[256,256]{0,1:T(8,128)}, u32[]{:S(2)}) copy-start(f32[256,256]{0,1:T(8,128)} %copy.105) | copy-start | bytes 786436
  217.0 45.8 %copy-start.1 = (bf16[1,2048,512]{2,1,0:T(8,128)(2,1)S(1)}, bf16[1,2048,512]{2,1,0:T(8,128)(2,1)}, u32[]{:S(2)}) copy-start(bf16[1,2048,512]{2,1,0:T(8,128)(2,1)} %param.20) | copy-start | bytes 6291460
  (12 other events, 17.5 us)
Sparse Core Ops, SparseCore 0:
  152.1 14.7 all-gather.1
  198.7 62.2 reduce-scatter.1
where the time goes:
time: 271 us; the launch traced here: 270 us
  Pallas kernels  85.2 us (31%)
  waiting for transfers between devices  53.7 us (20%)
  local copies, waits for them, and re-layouts  52.9 us (20%)
  matrix products  29.5 us (11%)
  other arithmetic  19.6 us (7%)
  between operations  16.3 us (6%)
  starting transfers between devices  12.4 us (5%)
    pallas_call x1, Pallas kernels, dispatch(): pl.pallas_call(kernel, name='dispatch', out_shape=(full, full), in_specs=...  53.9 us
    reduce_scatter x1, waiting for transfers between devices, on_device(): lax.psum_scatter(proj_part, 'sp', scatter_dimension=0, tiled=True)  39.1 us
    pallas_call x1, Pallas kernels, scatter_sum(): pl.pallas_call(kernel, name='scatter_sum', out_shape=jax.ShapeDtypeStruct...  24.7 us
    all_to_all x1, waiting for transfers between devices, on_device(): lax.all_to_all(row_grad.reshape(experts, capacity, width_dev), 'sp', spli...  14.6 us
    unnamed x124, local copies, waits for them, and re-layouts  13.8 us
    all_to_all x1, starting transfers between devices, on_device(): lax.all_to_all(row_grad.reshape(experts, capacity, width_dev), 'sp', spli...  12.1 us
    slice x58, local copies, waits for them, and re-layouts, on_device(): lax.associative_scan(combine_pair, (decay_fwd, decay_fwd * lru_grad), rev...  11.6 us
    slice x53, local copies, waits for them, and re-layouts, on_device(): lax.associative_scan(combine_pair, (decay_bwd, decay_bwd * lru_grad), axi...  6.68 us
  transfers between devices with their start and end apart: 3, of which 2 were waited for; matrix products, arithmetic and copies ran while one was open for 19% of the time, Pallas kernels for 2%

commit v1 on v0

--- a/solution.py
+++ b/solution.py
@@ -394,9 +394,10 @@
         full_residual, mix, (((0,), (1,)), ((), ())), preferred_element_type=jnp.float32
     ).astype(jnp.bfloat16)
     proj_part, full_residual = lax.optimization_barrier((proj_part, full_residual))
-    proj_rows = lax.psum_scatter(proj_part, "sp", scatter_dimension=0, tiled=True).astype(
-        jnp.float32
-    )
+    proj_blocks = lax.all_to_all(
+        proj_part.reshape(experts, -1, proj_part.shape[1]), "sp", split_axis=0, concat_axis=0, tiled=True
+    )
+    proj_rows = jnp.sum(proj_blocks.astype(jnp.float32), axis=0)
     out_proj_grad = proj_rows.T
     mix_grad = lax.dot_general(
         out_proj, full_residual, (((1,), (1,)), ((), ())), preferred_element_type=jnp.float32

time: 271 us -> 263 us (0.970)
  waiting for transfers between devices: 53.7 us -> 14.6 us
  local copies, waits for them, and re-layouts: 52.9 us -> 66.3 us
  Pallas kernels: 85.2 us -> 92.9 us
  other arithmetic: 19.6 us -> 26.8 us
  starting transfers between devices: 12.4 us -> 15.7 us
    reduce_scatter x1 -> x0, waiting for transfers between devices: 39.1 us -> none  [on_device(): lax.psum_scatter(proj_part, 'sp', scatter_dimension=0, tiled=True)]
    pallas_call x1, Pallas kernels: 6.65 us -> 14.4 us  [share(): pl.pallas_call(kernel, name='share', out_shape=jax.ShapeDtypeStruct((n,)...]
    all_to_all x0 -> x1, starting transfers between devices: none -> 3.57 us  [on_device(): lax.all_to_all(proj_part.reshape(experts, -1, proj_part.shape[1]), 'sp',...]
    add x18, other arithmetic: 0.2 us -> 3.32 us  [on_device(): lax.associative_scan(combine_pair, (decay_fwd, decay_fwd * lru_grad), rev...]
    pad x28, local copies, waits for them, and re-layouts: 0.42 us -> 3.27 us  [on_device(): lax.associative_scan(combine_pair, (decay_fwd, decay_fwd * lru_grad), rev...]
    slice x2, local copies, waits for them, and re-layouts: 0.07 us -> 2.88 us  [on_device(): carried_bwd[:, :-1]]
    rev x2, local copies, waits for them, and re-layouts: 0.26 us -> 3.06 us  [on_device(): lax.associative_scan(combine_pair, (decay_fwd, decay_fwd * lru_grad), rev...]
    unnamed x124 -> x108, local copies, waits for them, and re-layouts: 13.8 us -> 16.1 us
  transfers between devices with their start and end apart: 3 -> 3, of which waited for: 2 -> 1; matrix products, arithmetic and copies ran while one was open for 19% -> 28% of each run, Pallas kernels for 2% -> 5%
where the time goes in v1:
time: 263 us; the launch traced here: 261 us
  Pallas kernels  92.9 us (35%)
  local copies, waits for them, and re-layouts  66.3 us (25%)
  matrix products  29.1 us (11%)
  other arithmetic  26.8 us (10%)
  between operations  16 us (6%)
  starting transfers between devices  15.7 us (6%)
  waiting for transfers between devices  14.6 us (6%)
    pallas_call x1, Pallas kernels, dispatch(): pl.pallas_call(kernel, name='dispatch', out_shape=(full, full), in_specs=...  53.9 us
    pallas_call x1, Pallas kernels, scatter_sum(): pl.pallas_call(kernel, name='scatter_sum', out_shape=jax.ShapeDtypeStruct...  24.7 us
    unnamed x108, local copies, waits for them, and re-layouts  16.1 us
    all_to_all x1, waiting for transfers between devices, on_device(): lax.all_to_all(row_grad.reshape(experts, capacity, width_dev), 'sp', spli...  14.6 us
    pallas_call x1, Pallas kernels, share(): pl.pallas_call(kernel, name='share', out_shape=jax.ShapeDtypeStruct((n,)...  14.4 us
    slice x58, local copies, waits for them, and re-layouts, on_device(): lax.associative_scan(combine_pair, (decay_fwd, decay_fwd * lru_grad), rev...  12.2 us
    all_to_all x1, starting transfers between devices, on_device(): lax.all_to_all(row_grad.reshape(experts, capacity, width_dev), 'sp', spli...  12.1 us
    slice x53, local copies, waits for them, and re-layouts, on_device(): lax.associative_scan(combine_pair, (decay_bwd, decay_bwd * lru_grad), axi...  6.83 us
  transfers between devices with their start and end apart: 3, of which 1 were waited for; matrix products, arithmetic and copies ran while one was open for 28% of the time, Pallas kernels for 5%

profile of v1, /device:TPU:0, one launch (start us, length us, event | category | flops | bytes accessed | tf_op | source)
XLA Modules:
  0.0 261.5 jit_solution(13243403160919716500)
XLA Ops:
  13.4 1.7 mul.648
  15.4 3.8 %scatter_custom_fusion = bf16[768,512]{1,0:T(8,128)(2,1)} fusion(s32[512]{0:T(512)S(1)} %bitcast.328, bf16[512,512]{1,0:T(8,128)(2,1)} %reshape.587, bf16[]{:T(256)} %constant.22.clone.1), kind=kCustom, calls=%fused_computation.63 | custom fusion | bytes 786944 | tf_op jit(solution)/shard_map/scatter | solution.py:361
  19.3 3.5 %scatter_custom_fusion.1 = bf16[768,512]{1,0:T(8,128)(2,1)S(1)} fusion(s32[512]{0:T(512)S(1)} %bitcast.329, f32[512,512]{1,0:T(8,128)} %mul.648, f32[512]{0:T(512)S(1)} %mul.649, bf16[]{:T(256)} %constant.22.clone.1), kind=kCustom, calls=%fused_computation.52 | custom fusion | flops 524288 | bytes 1837058 | tf_op jit(solution)/shard_map/scatter | solution.py:362
  23.9 53.9 %dispatch.1 = (bf16[8,96,2048]{2,1,0:T(8,128)(2,1)S(1)}, bf16[8,96,2048]{2,1,0:T(8,128)(2,1)}) custom-call(bf16[8,96,512]{2,1,0:T(8,128)(2,1)S(1)} %bitcast.305, bf16[8,96,512]{2,1,0:T(8,128)(2,1)S(1)} %bitcast.304), custom_call_target="tpu_custom_call" | custom-call | tf_op jit(solution)/shard_map/dispatch/pallas_call | solution.py:139
  77.9 1.8 fusion.5
  80.6 1.8 fusion.8
  84.3 2.3 multiply_convert_fusion.1
  86.6 1.8 fusion.3
  88.5 1.8 add_convert_fusion.part_ref
  90.3 24.7 %scatter_sum.1 = bf16[768,512]{1,0:T(8,128)(2,1)} custom-call(bf16[768,2048]{1,0:T(8,128)(2,1)S(1)} %add_convert_fusion.part_ref), custom_call_target="tpu_custom_call" | custom-call | tf_op jit(solution)/shard_map/scatter_sum/pallas_call | solution.py:212
  115.0 12.1 %all-to-all-start = ((bf16[8,96,512]{2,1,0:T(8,128)(2,1)}), bf16[8,96,512]{2,1,0:T(8,128)(2,1)S(1)}, u32[]{:S(2)}, u32[]{:S(2)}) async-start(bf16[8,96,512]{2,1,0:T(8,128)(2,1)} %bitcast.14), calls=%async_computation | async-start | bytes 1572864 | tf_op jit(solution)/shard_map/all_to_all | solution.py:372
  132.7 14.6 %all-to-all-done = bf16[8,96,512]{2,1,0:T(8,128)(2,1)S(1)} async-done(((bf16[8,96,512]{2,1,0:T(8,128)(2,1)}), bf16[8,96,512]{2,1,0:T(8,128)(2,1)S(1)}, u32[]{:S(2)}, u32[]{:S(2)}) %all-to-all-start) | async-done | bytes 786464 | tf_op jit(solution)/shard_map/all_to_all | solution.py:372
  147.2 2.0 gather_fusion
  152.0 2.5 fusion.51
  154.5 1.6 slice.738
  156.1 1.6 slice.703
  157.7 1.6 slice.704
  160.1 1.6 slice.630
  161.7 1.6 slice.623
  163.3 1.6 slice.621
  165.6 1.7 copy.124
  167.2 1.5 slice.631
  168.8 1.5 slice.624
  170.3 1.5 slice.622
  171.8 4.4 %fusion = bf16[1,2048,512]{2,1,0:T(8,128)(2,1)} fusion(bf16[768,2048]{1,0:T(8,128)(2,1)S(1)} %bitcast.309, bf16[768,512]{1,0:T(8,128)(2,1)} %copy-done.22), kind=kOutput, calls=%fused_computation.7 | convolution fusion | flops 1611661312 | bytes 6029312 | tf_op jit(solution)/shard_map/dot_general | solution.py:315
  176.2 3.2 %fusion.1 = bf16[1,2048,512]{2,1,0:T(8,128)(2,1)} fusion(bf16[768,2048]{1,0:T(8,128)(2,1)S(1)} %bitcast.310, bf16[768,512]{1,0:T(8,128)(2,1)S(1)} %copy-done.21), kind=kOutput, calls=%fused_computation.8 | convolution fusion | flops 1611661312 | bytes 6029312 | tf_op jit(solution)/shard_map/dot_general | solution.py:318
  179.4 3.3 %fusion.2 = bf16[1,512,2048]{2,1,0:T(8,128)(2,1)} fusion(bf16[768,2048]{1,0:T(8,128)(2,1)S(1)} %bitcast.365, f32[768,512]{1,0:T(8,128)S(1)} %copy-done.47, f32[768,512]{1,0:T(8,128)S(1)} %copy-done.45), kind=kOutput, calls=%fused_computation.9 | convolution fusion | flops 1614020608 | bytes 8388608 | tf_op jit(solution)/shard_map/dot_general | solution.py:321
  182.7 2.9 %convolution_convert_fusion.3 = bf16[2048,256]{1,0:T(8,128)(2,1)} fusion(bf16[256,2048]{1,0:T(8,128)(2,1)} %all-gather.2.cloned.1.call-done, f32[256,256]{0,1:T(8,128)S(1)} %copy-done.28, bf16[256,256]{0,1:T(8,128)(2,1)S(1)} %copy-done.35), kind=kOutput, calls=%fused_computation.10 | convolution fusion | flops 269680640 | bytes 2490368 | tf_op jit(solution)/shard_map/dot_general | solution.py:393
  185.7 1.3 exponential_multiply_fusion.1
  189.8 1.4 pad.331
  191.2 1.5 pad.258
  192.7 1.4 pad.329
  194.2 1.4 pad.242
  197.5 3.6 %all-to-all-start.1 = ((bf16[8,256,256]{2,1,0:T(8,128)(2,1)}), bf16[8,256,256]{2,1,0:T(8,128)(2,1)S(1)}, u32[]{:S(2)}, u32[]{:S(2)}) async-start(bf16[8,256,256]{2,1,0:T(8,128)(2,1)} %bitcast.313), calls=%async_computation.1 | async-start | bytes 2097152 | tf_op jit(solution)/shard_map/all_to_all | solution.py:397
  201.0 1.5 pad.462
  202.5 1.4 pad.463
  204.7 1.5 pad.211
  207.0 1.7 add_multiply_fusion.2
  209.9 1.5 pad.226
  214.2 14.4 %share.1 = f32[8,1,1024]{2,1,0:T(1,128)S(1)} custom-call(f32[1,1024]{1,0:T(1,128)S(1)} %bitcast.306), custom_call_target="tpu_custom_call" | custom-call | tf_op jit(solution)/shard_map/share/pallas_call | solution.py:243
  228.8 1.3 multiply_add_fusion
  233.7 1.8 convolution_add_fusion
  237.3 1.8 copy.148
  239.1 1.7 rev.8
  240.9 1.3 rev.9
  247.8 2.2 add_add_fusion
  250.1 1.8 copy.150
  251.8 1.8 copy.151
  (403 shorter events, 41.2 us)
Async XLA Ops:
  7.2 70.7 %copy-start = (bf16[1,2048,512]{2,1,0:T(8,128)(2,1)S(1)}, bf16[1,2048,512]{2,1,0:T(8,128)(2,1)}, u32[]{:S(2)}) copy-start(bf16[1,2048,512]{2,1,0:T(8,128)(2,1)} %param.20) | copy-start | bytes 6291460
  7.2 5.9 %copy-start.18 = (bf16[256,512]{1,0:T(8,128)(2,1)S(1)}, bf16[256,512]{1,0:T(8,128)(2,1)}, u32[]{:S(2)}) copy-start(bf16[256,512]{1,0:T(8,128)(2,1)} %param.16) | copy-start | bytes 786436
  12.1 3.0 %copy-start.37 = (f32[256,2]{0,1:T(2,128)S(1)}, f32[256,2]{0,1:T(2,128)}, u32[]{:S(2)}) copy-start(f32[256,2]{0,1:T(2,128)} %param.19) | copy-start | bytes 6148
  77.9 1.8 copy-start.3
  77.9 2.7 %copy-start.14 = (bf16[1,2048,512]{2,1,0:T(8,128)(2,1)S(1)}, bf16[1,2048,512]{2,1,0:T(8,128)(2,1)}, u32[]{:S(2)}) copy-start(bf16[1,2048,512]{2,1,0:T(8,128)(2,1)} %param.21) | copy-start | bytes 6291460
  80.6 1.8 copy-start.44
  80.6 2.5 copy-start.39
  80.6 3.7 %copy-start.41 = (bf16[1,512,2048]{2,1,0:T(8,128)(2,1)S(1)}, bf16[1,512,2048]{2,1,0:T(8,128)(2,1)}, u32[]{:S(2)}) copy-start(bf16[1,512,2048]{2,1,0:T(8,128)(2,1)} %param.22) | copy-start | bytes 6291460
  82.4 4.2 %copy-start.46 = (f32[768,512]{1,0:T(8,128)}, f32[768,512]{1,0:T(8,128)S(1)}, u32[]{:S(2)}) copy-start(f32[768,512]{1,0:T(8,128)S(1)} %fusion.8) | copy-start | bytes 4718596
  86.6 1.9 copy-start.22
  86.6 1.8 copy-start.20
  90.3 36.9 %copy-start.34 = (bf16[256,256]{1,0:T(8,128)(2,1)S(1)}, bf16[256,256]{1,0:T(8,128)(2,1)}, u32[]{:S(2)}) copy-start(bf16[256,256]{1,0:T(8,128)(2,1)} %param.24) | copy-start | bytes 393220
  90.3 36.9 %copy-start.36 = (bf16[2,4,64,64]{3,2,1,0:T(8,128)(2,1)S(1)}, bf16[2,4,64,64]{3,2,1,0:T(8,128)(2,1)}, u32[]{:S(2)}) copy-start(bf16[2,4,64,64]{3,2,1,0:T(8,128)(2,1)} %param.30) | copy-start | bytes 196612
  115.0 13.0 %copy-start.29 = (f32[256,256]{1,0:T(8,128)S(1)}, f32[256,256]{1,0:T(8,128)}, u32[]{:S(2)}) copy-start(f32[256,256]{1,0:T(8,128)} %param.27) | copy-start | bytes 786436
  115.0 32.3 %all-to-all-start = ((bf16[8,96,512]{2,1,0:T(8,128)(2,1)}), bf16[8,96,512]{2,1,0:T(8,128)(2,1)S(1)}, u32[]{:S(2)}, u32[]{:S(2)}) async-start(bf16[8,96,512]{2,1,0:T(8,128)(2,1)} %bitcast.14), calls=%async_computation | async-start | bytes 1572864 | tf_op jit(solution)/shard_map/all_to_all | solution.py:372
  127.1 2.6 copy-start.30
  127.1 55.6 %all-gather.2.cloned.1.call-start = ((), (), s32[]{:S(2)}) async-start(), calls=%async_computation.2 | async-start | bytes 1310720 | tf_op jit(solution)/shard_map/all_gather | solution.py:385
  127.2 3.3 %copy-start.31 = (f32[256,256]{1,0:T(8,128)S(1)}, f32[256,256]{1,0:T(8,128)}, u32[]{:S(2)}) copy-start(f32[256,256]{1,0:T(8,128)} %param.28) | copy-start | bytes 786436
  127.5 3.2 %copy-start.32 = (bf16[2,4,64,64]{3,2,1,0:T(8,128)(2,1)S(1)}, bf16[2,4,64,64]{3,2,1,0:T(8,128)(2,1)}, u32[]{:S(2)}) copy-start(bf16[2,4,64,64]{3,2,1,0:T(8,128)(2,1)} %param.29) | copy-start | bytes 196612
  129.7 1.8 copy-start.38
  131.1 18.1 %copy-start.12 = (f32[256,256]{0,1:T(8,128)}, f32[256,256]{0,1:T(8,128)S(1)}, u32[]{:S(2)}) copy-start(f32[256,256]{0,1:T(8,128)S(1)} %copy.119) | copy-start | bytes 786436
  131.5 15.7 %copy-start.10 = (f32[256,256]{0,1:T(8,128)}, f32[256,256]{0,1:T(8,128)S(1)}, u32[]{:S(2)}) copy-start(f32[256,256]{0,1:T(8,128)S(1)} %copy.112) | copy-start | bytes 786436
  149.2 1.9 copy-start.19
  152.0 19.8 %copy-start.4 = (bf16[8,96,2048]{2,1,0:T(8,128)(2,1)S(1)}, bf16[8,96,2048]{2,1,0:T(8,128)(2,1)}, u32[]{:S(2)}) copy-start(bf16[8,96,2048]{2,1,0:T(8,128)(2,1)} %copy-done.3) | copy-start | bytes 9437188
  171.8 4.4 %copy-start.21 = (bf16[768,512]{1,0:T(8,128)(2,1)S(1)}, bf16[768,512]{1,0:T(8,128)(2,1)}, u32[]{:S(2)}) copy-start(bf16[768,512]{1,0:T(8,128)(2,1)} %copy-done.20) | copy-start | bytes 2359300
  176.2 3.2 %copy-start.40 = (bf16[8,96,2048]{2,1,0:T(8,128)(2,1)S(1)}, bf16[8,96,2048]{2,1,0:T(8,128)(2,1)}, u32[]{:S(2)}) copy-start(bf16[8,96,2048]{2,1,0:T(8,128)(2,1)} %get-tuple-element.12) | copy-start | bytes 9437188
  176.2 3.2 %copy-start.45 = (f32[768,512]{1,0:T(8,128)S(1)}, f32[768,512]{1,0:T(8,128)}, u32[]{:S(2)}) copy-start(f32[768,512]{1,0:T(8,128)} %copy-done.44) | copy-start | bytes 4718596
  176.2 3.2 %copy-start.47 = (f32[768,512]{1,0:T(8,128)S(1)}, f32[768,512]{1,0:T(8,128)}, u32[]{:S(2)}) copy-start(f32[768,512]{1,0:T(8,128)} %copy-done.46) | copy-start | bytes 4718596
  179.3 3.3 %copy-start.28 = (f32[256,256]{0,1:T(8,128)S(1)}, f32[256,256]{0,1:T(8,128)}, u32[]{:S(2)}) copy-start(f32[256,256]{0,1:T(8,128)} %fusion.51) | copy-start | bytes 786436
  179.4 3.3 %copy-start.35 = (bf16[256,256]{0,1:T(8,128)(2,1)S(1)}, bf16[256,256]{0,1:T(8,128)(2,1)}, u32[]{:S(2)}) copy-start(bf16[256,256]{0,1:T(8,128)(2,1)} %copy.124) | copy-start | bytes 393220
  182.7 3.0 %copy-start.9 = (f32[256,256]{0,1:T(8,128)S(1)}, f32[256,256]{0,1:T(8,128)}, u32[]{:S(2)}) copy-start(f32[256,256]{0,1:T(8,128)} %get-tuple-element.56) | copy-start | bytes 786436
  182.7 3.0 %copy-start.42 = (bf16[256,2048]{1,0:T(8,128)(2,1)S(1)}, bf16[256,2048]{1,0:T(8,128)(2,1)}, u32[]{:S(2)}) copy-start(bf16[256,2048]{1,0:T(8,128)(2,1)} %param.23) | copy-start | bytes 3145732
  182.7 2.9 %copy-start.43 = (bf16[256,2048]{1,0:T(8,128)(2,1)S(1)}, bf16[256,2048]{1,0:T(8,128)(2,1)}, u32[]{:S(2)}) copy-start(bf16[256,2048]{1,0:T(8,128)(2,1)} %all-gather.2.cloned.1.call-done) | copy-start | bytes 3145732
  185.7 1.6 copy-start.25
  185.7 1.6 copy-start.26
  187.0 1.8 copy-start.15
  189.6 6.7 %copy-start.23 = (f32[256,128]{0,1:T(8,128)S(1)}, f32[256,128]{0,1:T(8,128)}, u32[]{:S(2)}) copy-start(f32[256,128]{0,1:T(8,128)} %slice.631) | copy-start | bytes 393220
  189.6 6.7 %copy-start.24 = (f32[256,128]{0,1:T(8,128)S(1)}, f32[256,128]{0,1:T(8,128)}, u32[]{:S(2)}) copy-start(f32[256,128]{0,1:T(8,128)} %slice.624) | copy-start | bytes 393220
  197.5 56.2 %all-to-all-start.1 = ((bf16[8,256,256]{2,1,0:T(8,128)(2,1)}), bf16[8,256,256]{2,1,0:T(8,128)(2,1)S(1)}, u32[]{:S(2)}, u32[]{:S(2)}) async-start(bf16[8,256,256]{2,1,0:T(8,128)(2,1)} %bitcast.313), calls=%async_computation.1 | async-start | bytes 2097152 | tf_op jit(solution)/shard_map/all_to_all | solution.py:397
  207.0 23.1 %copy-start.8 = (f32[256,256]{0,1:T(8,128)S(1)}, f32[256,256]{0,1:T(8,128)}, u32[]{:S(2)}) copy-start(f32[256,256]{0,1:T(8,128)} %copy.121) | copy-start | bytes 786436
  207.0 23.1 %copy-start.13 = (f32[256,256]{0,1:T(8,128)S(1)}, f32[256,256]{0,1:T(8,128)}, u32[]{:S(2)}) copy-start(f32[256,256]{0,1:T(8,128)} %copy-done.12) | copy-start | bytes 786436
  208.8 21.2 %copy-start.17 = (f32[256,256]{0,1:T(8,128)}, f32[256,256]{0,1:T(8,128)S(1)}, u32[]{:S(2)}) copy-start(f32[256,256]{0,1:T(8,128)S(1)} %pad.227) | copy-start | bytes 786436
  228.7 3.6 %copy-start.33 = (bf16[2,4,64,64]{3,2,1,0:T(8,128)(2,1)S(1)}, bf16[2,4,64,64]{3,2,1,0:T(8,128)(2,1)}, u32[]{:S(2)}) copy-start(bf16[2,4,64,64]{3,2,1,0:T(8,128)(2,1)} %param.29) | copy-start | bytes 196612
  230.1 5.5 %copy-start.16 = (f32[256,256]{0,1:T(8,128)S(1)}, f32[256,256]{0,1:T(8,128)}, u32[]{:S(2)}) copy-start(f32[256,256]{0,1:T(8,128)} %pad.211) | copy-start | bytes 786436
  235.5 7.7 %copy-start.5 = (f32[256,256]{0,1:T(8,128)S(1)}, f32[256,256]{0,1:T(8,128)}, u32[]{:S(2)}) copy-start(f32[256,256]{0,1:T(8,128)} %copy.116) | copy-start | bytes 786436
  235.5 7.7 %copy-start.7 = (f32[256,256]{0,1:T(8,128)S(1)}, f32[256,256]{0,1:T(8,128)}, u32[]{:S(2)}) copy-start(f32[256,256]{0,1:T(8,128)} %copy.114) | copy-start | bytes 786436
  235.5 7.8 %copy-start.11 = (f32[256,256]{0,1:T(8,128)S(1)}, f32[256,256]{0,1:T(8,128)}, u32[]{:S(2)}) copy-start(f32[256,256]{0,1:T(8,128)} %copy-done.10) | copy-start | bytes 786436
  247.8 6.8 %copy-start.1 = (bf16[1,2048,512]{2,1,0:T(8,128)(2,1)S(1)}, bf16[1,2048,512]{2,1,0:T(8,128)(2,1)}, u32[]{:S(2)}) copy-start(bf16[1,2048,512]{2,1,0:T(8,128)(2,1)} %param.20) | copy-start | bytes 6291460
  (4 other events, 4.1 us)
Sparse Core Ops, SparseCore 0:
  152.1 14.7 all-gather.1
